TPU v7x, 32 devices: a whole 2x2x4 slice. The times are simulated.
32 devices in a mesh: sp: 8 (over z, x), tp: 4 (over y, core).
Axes of the slice: x: 2, y: 2, z: 4, core: 2. Of those that a mesh axis runs over, the one named last changes fastest.
Arguments:
- resid: bfloat16 [1024, 2048], P('sp'), may hold values from -6 to 6
- norm_gain: float32 [2048], replicated, may hold values from 0.1 to 1.9
- cotangent: bfloat16 [1024, 2048], P('sp'), may hold values from -6 to 6
- route_ids: int32 [1024, 2], P('sp'), may hold values from 0 to 7, all different within a row; in each aligned block of 128 rows (0 to 127, 128 to 255, ...) at most 48 rows name the same one
- route_weight: float32 [1024, 2], P('sp'), may hold values from 0.25 to 2.25
- expert_gate: bfloat16 [8, 2048, 2048], P('sp', None, 'tp'), may hold values from -0.125 to 0.125
- expert_up: bfloat16 [8, 2048, 2048], P('sp', None, 'tp'), may hold values from -0.125 to 0.125
- expert_down: bfloat16 [8, 2048, 2048], P('sp', 'tp'), may hold values from -0.125 to 0.125
- out_proj: bfloat16 [2048, 4096], P('sp', 'tp'), may hold values from -0.09375 to 0.09375
- mixed: bfloat16 [1024, 4096], P('sp', 'tp'), may hold values from -6 to 6
- query: bfloat16 [1024, 2048], P('sp', 'tp'), may hold values from -6 to 6
- key: bfloat16 [1024, 2048], P('sp', 'tp'), may hold values from -1.5 to 1.5
- value: bfloat16 [1024, 4096], P('sp', 'tp'), may hold values from -6 to 6
- log_decay: float32 [1024, 2048], P('sp', 'tp'), may hold values from -1 to 0, as said below
- span_state: float32 [8, 16, 128, 256], P('sp', 'tp'), may hold values from -24 to 24
Outputs:
- grad_expert_gate: bfloat16 [8, 2048, 2048], P('sp', None, 'tp')
- grad_expert_up: bfloat16 [8, 2048, 2048], P('sp', None, 'tp')
- grad_expert_down: bfloat16 [8, 2048, 2048], P('sp', 'tp')
- grad_out_proj: float32 [2048, 4096], P('sp', 'tp')
- grad_query: bfloat16 [1024, 2048], P('sp', 'tp')
- grad_key: bfloat16 [1024, 2048], P('sp', 'tp')
- grad_value: bfloat16 [1024, 4096], P('sp', 'tp')
- grad_log_decay: float32 [1024, 2048], P('sp', 'tp')
Inputs may be any that keep to these rules, and one draw needn't show every extreme that they name: `route_ids`: A row names 2 different experts. Within each aligned block of 128 rows (the rows of one index of sp) no expert is named by more than 48 rows, and in every draw some expert is named by exactly 48 rows of some block. `log_decay`: every entry is zero or negative.
All inputs are finite; a program needn't handle non-finite values.
Results may differ from a plain program's by a relative error of at most 0.023.
Values may be sent and summed in bfloat16 or wider, within the bound.
A program may use at most 128 MiB of HBM per device.

v0:
```python
import jax
import jax.numpy as jnp
from jax import lax
from jax.sharding import PartitionSpec as P

KEY_CHANNELS = 128
DV = 256
TOP = 2
BLOCK = 64


epsilon = 1e-06
highest = lax.Precision.HIGHEST


def entering(array, axis, join, neutral):
    count = lax.axis_size(axis)
    place = lax.axis_index(axis)
    ahead = count - 1 - place
    gathered = jax.tree.map(
        lambda a, kind: lax.all_gather(a.astype(kind), axis), array, (jnp.bfloat16, jnp.bfloat16)
    )
    state = jax.tree.map(lambda a, e: jnp.zeros_like(a) + jnp.asarray(e, a.dtype), array, neutral)

    def one(lap, state):
        source = count - 1 - lap
        return join(
            state,
            jax.tree.map(
                lambda a, own: lax.dynamic_index_in_dim(a, source, 0, False).astype(own.dtype),
                gathered,
                array,
            ),
        )

    return lax.fori_loop(0, ahead, one, state)


def into_blocks(values):
    return values.reshape(values.shape[0] // BLOCK, BLOCK, values.shape[1])


def span_forward(query_rows, key_rows, value_rows, grad_rows, decay_rows, entry_state):
    query_blk = into_blocks(query_rows)
    key_blk = into_blocks(key_rows)
    value_blk = into_blocks(value_rows)
    grad_blk = into_blocks(grad_rows)
    cumlog = jnp.cumsum(into_blocks(decay_rows), axis=1)
    block_total = cumlog[:, -1, :]
    to_end = jnp.exp(block_total[:, None, :] - cumlog)
    inner_part = jnp.einsum("nsd,nsj->ndj", key_blk * to_end, value_blk, precision=highest)

    def forward_step(carry_state, step_item):
        piece_part, block_sum = step_item
        return (jnp.exp(block_sum)[:, None] * carry_state + piece_part, carry_state)

    end_state, starts = lax.scan(forward_step, entry_state, (inner_part, block_total))
    own_part = jnp.einsum("ntd,ntj->ndj", query_blk * jnp.exp(cumlog), grad_blk, precision=highest)

    def backward_step(carry_state, step_item):
        piece_part, block_sum = step_item
        return (jnp.exp(block_sum)[:, None] * carry_state + piece_part, carry_state)

    start_cot, after_cot = lax.scan(
        backward_step, jnp.zeros_like(entry_state), (own_part, block_total), reverse=True
    )
    span_total = jnp.sum(block_total, axis=0)
    later_log = span_total[None, :] - jnp.cumsum(block_total, axis=0)
    return ((cumlog, starts, after_cot, later_log, end_state), (jnp.exp(span_total), start_cot))


def span_backward(query_rows, key_rows, value_rows, grad_rows, kept_terms, exit_cot):
    cumlog, starts, after_cot, later_log, end_state = kept_terms
    query_blk = into_blocks(query_rows)
    key_blk = into_blocks(key_rows)
    value_blk = into_blocks(value_rows)
    grad_blk = into_blocks(grad_rows)
    exit_cots = after_cot + jnp.exp(later_log)[:, :, None] * exit_cot
    causal = jnp.arange(BLOCK)[:, None] >= jnp.arange(BLOCK)[None, :]
    decays = jnp.exp(
        jnp.where(causal[None, :, :, None], cumlog[:, :, None, :] - cumlog[:, None, :, :], -jnp.inf)
    )
    scores = jnp.einsum("ntd,nsd,ntsd->nts", query_blk, key_blk, decays, precision=highest)
    grad_scores = jnp.einsum("ntj,nsj->nts", grad_blk, value_blk, precision=highest)
    grad_query = jnp.exp(cumlog) * jnp.einsum("ntj,ndj->ntd", grad_blk, starts, precision=highest)
    grad_query = grad_query + jnp.einsum(
        "nts,nsd,ntsd->ntd", grad_scores, key_blk, decays, precision=highest
    )
    to_end = jnp.exp(cumlog[:, -1:, :] - cumlog)
    grad_key = jnp.einsum("nts,ntd,ntsd->nsd", grad_scores, query_blk, decays, precision=highest)
    grad_key = grad_key + to_end * jnp.einsum(
        "nsj,ndj->nsd", value_blk, exit_cots, precision=highest
    )
    grad_value = jnp.einsum("nts,ntj->nsj", scores, grad_blk, precision=highest)
    grad_value = grad_value + jnp.einsum(
        "nsd,ndj->nsj", key_blk * to_end, exit_cots, precision=highest
    )
    length = query_rows.shape[0]
    key_width = query_rows.shape[1]
    per_position = (query_blk * grad_query - key_blk * grad_key).reshape(length, key_width)
    grad_log = (
        jnp.flip(jnp.cumsum(jnp.flip(per_position, 0), 0), 0)
        + jnp.sum(end_state * exit_cot, axis=1)[None, :]
    )
    return (
        grad_query.reshape(length, key_width),
        grad_key.reshape(length, key_width),
        grad_value.reshape(length, value_rows.shape[1]),
        grad_log,
    )


def join_later(earlier, later):
    return (earlier[0] * later[0], later[1] + later[0][..., None] * earlier[1])


def on_device(
    resid,
    norm_gain,
    cotangent,
    route_ids,
    route_weight,
    expert_gate,
    expert_up,
    expert_down,
    out_proj,
    mixed,
    query,
    key,
    value,
    log_decay,
    span_state,
):
    tokens_here = resid.shape[0]
    model_width = resid.shape[1]
    sp_count = lax.axis_size("sp")
    tp_count = lax.axis_size("tp")
    experts = sp_count * expert_gate.shape[0]
    capacity = 3 * tokens_here // experts
    resid_f = resid.astype(jnp.float32)
    inverse_rms = lax.rsqrt(jnp.mean(resid_f * resid_f, axis=1, keepdims=True) + epsilon)
    unit_rows = resid_f * inverse_rms
    normed = (unit_rows * norm_gain).astype(jnp.bfloat16)
    pair_expert = route_ids.reshape(-1)
    onehot = (pair_expert[:, None] == jnp.arange(experts, dtype=jnp.int32)[None, :]).astype(
        jnp.int32
    )
    slot_rank = jnp.sum((jnp.cumsum(onehot, axis=0) - onehot) * onehot, axis=1)
    slot_of = pair_expert * capacity + slot_rank
    slot_pairs = slot_of[None, :] == jnp.arange(experts * capacity, dtype=jnp.int32)[:, None]
    slot_tokens = jnp.any(slot_pairs.reshape(experts * capacity, tokens_here, TOP), axis=2).astype(
        jnp.bfloat16
    )
    slot_weight = jnp.sum(jnp.where(slot_pairs, route_weight.reshape(1, -1), 0.0), axis=1)
    column_share = model_width // tp_count
    offset = lax.axis_index("tp") * column_share
    rows_in = jnp.dot(
        slot_tokens,
        lax.dynamic_slice_in_dim(normed, offset, column_share, 1),
        preferred_element_type=jnp.float32,
    ).astype(jnp.bfloat16)
    rows_cot = (
        jnp.dot(
            slot_tokens,
            lax.dynamic_slice_in_dim(cotangent, offset, column_share, 1),
            preferred_element_type=jnp.float32,
        )
        * slot_weight[:, None]
    )
    arrived = (
        lax.all_to_all(
            rows_in.reshape(experts, capacity, -1), "sp", split_axis=0, concat_axis=1, tiled=True
        ),
        lax.all_to_all(
            rows_cot.astype(jnp.bfloat16).reshape(experts, capacity, -1),
            "sp",
            split_axis=0,
            concat_axis=1,
            tiled=True,
        ),
    )
    expert_in, expert_cot = (
        lax.all_gather(arrived[0], "tp", axis=2, tiled=True),
        lax.all_gather(arrived[1], "tp", axis=2, tiled=True),
    )
    gate_pre = jnp.einsum(
        "erd,edf->erf", expert_in, expert_gate, preferred_element_type=jnp.float32
    )
    up_pre = jnp.einsum("erd,edf->erf", expert_in, expert_up, preferred_element_type=jnp.float32)
    gate_sig = jax.nn.sigmoid(gate_pre)
    hidden = (gate_pre * gate_sig * up_pre).astype(jnp.bfloat16)
    grad_hidden = jnp.einsum(
        "erd,efd->erf", expert_cot, expert_down, preferred_element_type=jnp.float32
    )
    grad_up_act = (grad_hidden * gate_pre * gate_sig).astype(jnp.bfloat16)
    grad_gate_act = (grad_hidden * up_pre * gate_sig * (1.0 + gate_pre * (1.0 - gate_sig))).astype(
        jnp.bfloat16
    )
    grad_down_w = jnp.einsum("erf,erd->efd", hidden, expert_cot, preferred_element_type=jnp.float32)
    grad_gate_w = jnp.einsum(
        "erd,erf->edf", expert_in, grad_gate_act, preferred_element_type=jnp.float32
    )
    grad_up_w = jnp.einsum(
        "erd,erf->edf", expert_in, grad_up_act, preferred_element_type=jnp.float32
    )
    partial_value = jnp.einsum(
        "erf,edf->erd", grad_gate_act, expert_gate, preferred_element_type=jnp.float32
    )
    partial_value = partial_value + jnp.einsum(
        "erf,edf->erd", grad_up_act, expert_up, preferred_element_type=jnp.float32
    )
    partial_short = partial_value.astype(jnp.bfloat16)
    summed = (
        lax.psum_scatter(partial_short, "tp", scatter_dimension=2, tiled=True)
        .astype(jnp.float32)
        .astype(jnp.bfloat16)
    )
    returned = lax.all_to_all(summed, "sp", split_axis=1, concat_axis=0, tiled=True)
    flat_rows = returned.reshape(experts * capacity, -1)
    grad_normed = lax.all_gather(
        lax.dot_general(
            slot_tokens, flat_rows, (((0,), (0,)), ((), ())), preferred_element_type=jnp.float32
        ).astype(jnp.bfloat16),
        "tp",
        axis=1,
        tiled=True,
    ).astype(jnp.float32)
    scaled = grad_normed * norm_gain
    grad_resid = cotangent.astype(jnp.float32) + inverse_rms * (
        scaled - unit_rows * jnp.mean(scaled * unit_rows, axis=1, keepdims=True)
    )
    grad_resid = grad_resid.astype(jnp.bfloat16)
    resid_cols = grad_resid
    grad_out_proj = lax.psum_scatter(
        lax.dot_general(
            resid_cols, mixed, (((0,), (0,)), ((), ())), preferred_element_type=jnp.float32
        ).astype(jnp.bfloat16),
        "sp",
        scatter_dimension=0,
        tiled=True,
    ).astype(jnp.float32)
    resid_cols = grad_resid
    grad_mixed = jnp.dot(
        resid_cols,
        lax.all_gather(out_proj, "sp", axis=0, tiled=True),
        preferred_element_type=jnp.float32,
    ).astype(jnp.bfloat16)
    head_count = query.shape[1] // KEY_CHANNELS
    query_scale = KEY_CHANNELS ** (-0.5)

    def heads_first(values, head_depth):
        return values.reshape(tokens_here, head_count, head_depth).transpose(1, 0, 2)

    query_rows = heads_first(query, KEY_CHANNELS).astype(jnp.float32) * query_scale
    key_rows = heads_first(key, KEY_CHANNELS).astype(jnp.float32)
    value_rows = heads_first(value, DV).astype(jnp.float32)
    grad_rows = heads_first(grad_mixed, DV).astype(jnp.float32)
    decay_rows = heads_first(log_decay, KEY_CHANNELS)
    kept_terms, summary = jax.vmap(span_forward)(
        query_rows, key_rows, value_rows, grad_rows, decay_rows, span_state[0]
    )
    identity = (jnp.ones_like(summary[0]), jnp.zeros_like(summary[1]))
    carried = entering((summary[0], summary[1]), "sp", join_later, identity)
    head_grads = jax.vmap(span_backward)(
        query_rows, key_rows, value_rows, grad_rows, kept_terms, carried[1]
    )

    def tokens_first(values):
        return values.transpose(1, 0, 2).reshape(tokens_here, -1)

    grad_query = (tokens_first(head_grads[0]) * query_scale).astype(jnp.bfloat16)
    grad_key = tokens_first(head_grads[1]).astype(jnp.bfloat16)
    grad_value = tokens_first(head_grads[2]).astype(jnp.bfloat16)
    grad_log_decay = tokens_first(head_grads[3])
    return (
        grad_gate_w.astype(jnp.bfloat16),
        grad_up_w.astype(jnp.bfloat16),
        grad_down_w.astype(jnp.bfloat16),
        grad_out_proj,
        grad_query,
        grad_key,
        grad_value,
        grad_log_decay,
    )


def solution(mesh):
    return jax.shard_map(
        on_device,
        mesh=mesh,
        in_specs=(
            P("sp", None),
            P(),
            P("sp", None),
            P("sp", None),
            P("sp", None),
            P("sp", None, "tp"),
            P("sp", None, "tp"),
            P("sp", "tp", None),
            P("sp", "tp"),
            P("sp", "tp"),
            P("sp", "tp"),
            P("sp", "tp"),
            P("sp", "tp"),
            P("sp", "tp"),
            P("sp", "tp", None, None),
        ),
        out_specs=(
            P("sp", None, "tp"),
            P("sp", None, "tp"),
            P("sp", "tp", None),
            P("sp", "tp"),
            P("sp", "tp"),
            P("sp", "tp"),
            P("sp", "tp"),
            P("sp", "tp"),
        ),
        check_vma=False,
    )
```

profile of v0, /device:TPU:0, one launch (start us, length us, event | category | flops | bytes accessed | tf_op | source)
XLA Modules:
  0.0 320.2 jit_solution(13305534653315224760)
XLA Ops:
  15.0 19.2 %all_to_all.33 = bf16[8,48,512]{2,1,0:T(8,128)(2,1)} all-to-all(bf16[8,48,512]{2,1,0:T(8,128)(2,1)S(1)} %bitcast.230), channel_id=1, replica_groups=mesh['sp'=8,'tp'=4] {'sp'}, dimensions={0} | all-to-all | bytes 786432 | tf_op jit(solution)/shard_map/all_to_all | solution.py:171
  35.0 15.1 %all_to_all.34 = bf16[8,48,512]{2,1,0:T(8,128)(2,1)} all-to-all(bf16[8,48,512]{2,1,0:T(8,128)(2,1)S(1)} %bitcast.231), channel_id=1, replica_groups=mesh['sp'=8,'tp'=4] {'sp'}, dimensions={0} | all-to-all | bytes 786432 | tf_op jit(solution)/shard_map/all_to_all | solution.py:174
  50.2 2.6 all-gather.8.cloned.1.call-done
  52.7 4.0 %fusion.12 = f32[384,512]{1,0:T(8,128)} fusion(bf16[1,2048,512]{2,1,0:T(8,128)(2,1)} %param.27, bf16[1,384,2048]{2,1,0:T(8,128)(2,1)} %all-gather.8.cloned.1.call-done), kind=kOutput, calls=%fused_computation.29 | convolution fusion | flops 805306368 | bytes 4456448 | tf_op jit(solution)/shard_map/erd,edf->erf/dot_general | solution.py:189
  58.6 15.3 %all-gather.10.cloned.1.call-done = bf16[1,384,2048]{2,1,0:T(8,128)(2,1)} async-done(((bf16[1,384,512]{2,1,0:T(8,128)(2,1)}), bf16[1,384,2048]{2,1,0:T(8,128)(2,1)}) %all-gather.10.cloned.1.call-update) | async-done | bytes 1572880 | tf_op jit(solution)/shard_map/all_gather | solution.py:184
  74.0 3.7 %multiply_convert_fusion.1 = (bf16[384,512]{1,0:T(8,128)(2,1)S(1)}, bf16[384,512]{1,0:T(8,128)(2,1)S(1)}) fusion(f32[384,512]{1,0:T(8,128)} %fusion.9, f32[384,512]{1,0:T(8,128)} %fusion.12, bf16[1,512,2048]{2,1,0:T(8,128)(2,1)} %param.28, bf16[1,384,2048]{2,1,0:T(8,128)(2,1)} %all-gather.10.cloned.1.call-done), kind=kOutput, calls=%fused_computation.64 | convolution fusion | flops 807862272 | bytes 6029312 | tf_op jit(solution)/shard_map/erd,efd->erf/dot_general | solution.py:192
  82.3 27.6 %reduce-scatter.3.cloned.1.call-done = bf16[1,384,512]{2,1,0:T(8,128)(2,1)} async-done(((bf16[1,384,2048]{2,1,0:T(8,128)(2,1)}), bf16[1,384,512]{2,1,0:T(8,128)(2,1)}) %reduce-scatter.3.cloned.1.call-update) | async-done | bytes 393232 | tf_op jit(solution)/shard_map/reduce_scatter | solution.py:214
  112.0 3.0 reduce.9
  116.1 5.6 %all-to-all-start.2 = ((bf16[8,2,12288]{2,1,0:T(2,128)(2,1)}), bf16[8,2,12288]{2,1,0:T(2,128)(2,1)S(1)}, u32[]{:S(2)}, u32[]{:S(2)}) async-start(bf16[8,2,12288]{2,1,0:T(2,128)(2,1)} %reshape.320), calls=%async_computation.3 | async-start | bytes 786432 | tf_op jit(solution)/shard_map/all_to_all | solution.py:218
  123.5 21.2 %all-to-all-done.2 = bf16[8,2,12288]{2,1,0:T(2,128)(2,1)S(1)} async-done(((bf16[8,2,12288]{2,1,0:T(2,128)(2,1)}), bf16[8,2,12288]{2,1,0:T(2,128)(2,1)S(1)}, u32[]{:S(2)}, u32[]{:S(2)}) %all-to-all-start.2) | async-done | bytes 393248 | tf_op jit(solution)/shard_map/all_to_all | solution.py:218
  145.4 6.9 %all_gather.24 = bf16[128,2048]{1,0:T(8,128)(2,1)S(1)} all-gather(bf16[128,512]{1,0:T(8,128)(2,1)S(1)} %convolution_convert_fusion.6), channel_id=1, replica_groups=mesh['sp'=8,'tp'=4] {'tp'}, dimensions={1}, use_global_device_ids=true | all-gather | bytes 655360 | tf_op jit(solution)/shard_map/all_gather | solution.py:220
  153.3 10.2 %all-gather.12.cloned.1.call-done = bf16[2048,1024]{1,0:T(8,128)(2,1)} async-done(((bf16[256,1024]{1,0:T(8,128)(2,1)}), bf16[2048,1024]{1,0:T(8,128)(2,1)}) %all-gather.12.cloned.1.call-update) | async-done | bytes 4194320 | tf_op jit(solution)/shard_map/all_gather | solution.py:245
  163.5 3.1 convolution_convert_fusion.5
  174.3 19.4 %all-gather.2 = bf16[8,4,128]{2,1,0:T(4,128)(2,1)} all-gather(bf16[1,4,128]{2,1,0:T(4,128)(2,1)S(1)} %fusion.47), channel_id=3, replica_groups=mesh['sp'=8,'tp'=4] {'sp'}, dimensions={0}, use_global_device_ids=true | all-gather | bytes 9216 | tf_op jit(solution)/shard_map/all_gather | solution.py:21
  195.8 4.5 %convolution_convert_fusion = bf16[2048,1024]{1,0:T(8,128)(2,1)} fusion(bf16[128,1024]{1,0:T(8,128)(2,1)S(1)} %copy-done.25, bf16[128,2048]{1,0:T(8,128)(2,1)S(1)} %all_gather.24, bf16[128,2048]{1,0:T(8,128)(2,1)} %param.23, f32[128]{0:T(128)} %copy-done.30, f32[2048]{0:T(1024)S(1)} %copy-done.26, f32[128]{0:T(128)} %copy-done.29, ...), kind=kOutput, calls=%fused_computation.15 | convolution fusion | flops 541589504 | bytes 6038528 | tf_op jit(solution)/shard_map/dot_general | solution.py:235
  201.3 9.4 %fusion = (f32[4,2,64,64]{3,2,1,0:T(8,128)}, f32[4,2,64,128,64]{3,4,2,1,0:T(8,128)}) fusion(f32[4,2,128,64]{2,3,1,0:T(8,128)S(1)} %bitcast.214, f32[4,2,128,64]{2,3,1,0:T(8,128)S(1)} %bitcast.226, f32[4,2,64,128]{3,2,1,0:T(8,128)S(1)} %reduce_window_sum.50, pred[64,64]{1,0:T(8,128)(4,1)S(1)} %iota_compare_fusion.2), kind=kLoop, calls=%fused_computation.9 | loop fusion | flops 20938752 | bytes 17698816 | tf_op jit(solution)/shard_map/vmap(ntd,nsd,ntsd->nts)/dot_general | solution.py:83
  211.3 4.5 %fusion.4 = bf16[1,2048,512]{2,1,0:T(8,128)(2,1)} fusion(bf16[384,512]{1,0:T(8,128)(2,1)} %copy-done.21, bf16[1,384,2048]{2,1,0:T(8,128)(2,1)} %all-gather.8.cloned.1.call-done), kind=kOutput, calls=%fused_computation.21 | convolution fusion | flops 806354944 | bytes 4063232 | tf_op jit(solution)/shard_map/erd,erf->edf/dot_general | solution.py:203
  215.9 2.6 fusion.3
  218.5 2.7 fusion.5
  222.8 15.1 %fusion.1 = f32[4,2,64,128]{3,2,1,0:T(8,128)S(1)} fusion(f32[4,2,64,128,64]{3,4,2,1,0:T(8,128)} %get-tuple-element.416, f32[4,2,64,128]{3,2,1,0:T(8,128)S(1)} %bitcast.215, f32[4,2,64,64]{3,2,1,0:T(8,128)S(1)} %copy.217), kind=kLoop, calls=%fused_computation.11 | loop fusion | flops 12517376 | bytes 17432576 | tf_op jit(solution)/shard_map/vmap(nts,nsd,ntsd->ntd)/dot_general | solution.py:86
  239.4 6.3 %multiply_reduce_fusion = f32[4,2,64,128]{3,2,1,0:T(8,128)} fusion(f32[4,2,64,64]{3,2,1,0:T(8,128)S(1)} %fusion.51, f32[4,2,64,128]{3,2,1,0:T(8,128)S(1)} %bitcast.227, f32[4,2,64,128]{3,2,1,0:T(8,128)S(1)} %reduce_window_sum.50, pred[64,64]{1,0:T(8,128)(4,1)S(1)} %iota_compare_fusion.2), kind=kLoop, calls=%fused_computation.12 | loop fusion | flops 20905984 | bytes 921600 | tf_op jit(solution)/shard_map/vmap(nts,ntd,ntsd->nsd)/dot_general | solution.py:90
  245.8 12.8 %while.44 = (s32[]{:T(128)}, f32[4,128,256]{2,1,0:T(8,128)S(1)}, s32[]{:T(128)}, bf16[8,4,128,256]{3,2,1,0:T(8,128)(2,1)}, bf16[8,4,128]{2,1,0:T(4,128)(2,1)}, /*index=5*/s32[]{:T(128)}, s32[]{:T(128)}, s32[]{:T(128)}, s32[]{:T(128)}) while((s32[]{:T(128)}, f32[4,128,256]{2,1,0:T(8,128)S(1)}, s32[]{:T(128)}, ...), condition=%wide.region_17.18_spmd, body=%wide.region_16.17_spmd.sunk | while | flops 393734 | bytes 1315987 | solution.py:36
  258.6 2.7 multiply_subtract_fusion
  268.3 42.4 %reduce-scatter.5.cloned.1.call-done = bf16[256,1024]{1,0:T(8,128)(2,1)} async-done(((bf16[2048,1024]{1,0:T(8,128)(2,1)}), bf16[256,1024]{1,0:T(8,128)(2,1)}) %reduce-scatter.5.cloned.1.call-update) | async-done | bytes 524304 | tf_op jit(solution)/shard_map/reduce_scatter | solution.py:234
  (188 shorter events, 59.0 us)
Async XLA Ops:
  8.0 48.8 %copy-start = (bf16[1,2048,512]{2,1,0:T(8,128)(2,1)S(1)}, bf16[1,2048,512]{2,1,0:T(8,128)(2,1)}, u32[]{:S(2)}) copy-start(bf16[1,2048,512]{2,1,0:T(8,128)(2,1)} %param.26) | copy-start | bytes 6291460
  8.0 44.7 %all-gather.8.cloned.1.call-start = ((), (), s32[]{:S(2)}) async-start(), calls=%async_computation.5 | async-start | bytes 1966080 | tf_op jit(solution)/shard_map/all_gather | solution.py:183
  10.2 24.1 %copy-start.31 = (f32[128,2]{0,1:T(2,128)S(1)}, f32[128,2]{0,1:T(2,128)}, u32[]{:S(2)}) copy-start(f32[128,2]{0,1:T(2,128)} %param.25) | copy-start | bytes 3076
  10.5 24.2 %copy-start.9 = (bf16[128,2048]{1,0:T(8,128)(2,1)S(1)}, bf16[128,2048]{1,0:T(8,128)(2,1)}, u32[]{:S(2)}) copy-start(bf16[128,2048]{1,0:T(8,128)(2,1)} %param.23) | copy-start | bytes 1572868
  11.3 23.7 %copy-start.19 = (pred[384,128]{1,0:T(8,128)(4,1)}, pred[384,128]{1,0:T(8,128)(4,1)S(1)}, u32[]{:S(2)}) copy-start(pred[384,128]{1,0:T(8,128)(4,1)S(1)} %fusion.34) | copy-start | bytes 147460
  34.2 39.7 %all-gather.10.cloned.1.call-start = ((), (), s32[]{:S(2)}) async-start(), calls=%async_computation.6 | async-start | bytes 1966080 | tf_op jit(solution)/shard_map/all_gather | solution.py:184
  50.1 59.7 %reduce-scatter.3.cloned.1.call-start = ((), (), s32[]{:S(2)}) async-start(), calls=%async_computation.7 | async-start | bytes 1966080 | tf_op jit(solution)/shard_map/reduce_scatter | solution.py:214
  81.7 81.7 %all-gather.12.cloned.1.call-start = ((), (), s32[]{:S(2)}) async-start(), calls=%async_computation.9 | async-start | bytes 4718592 | tf_op jit(solution)/shard_map/all_gather | solution.py:245
  82.3 39.5 %copy-start.24 = (f32[128,512]{1,0:T(8,128)S(1)}, f32[128,512]{1,0:T(8,128)}, u32[]{:S(2)}) copy-start(f32[128,512]{1,0:T(8,128)} %param.34) | copy-start | bytes 786436
  112.0 10.8 %copy-start.17 = (bf16[128,512]{1,0:T(8,128)(2,1)S(1)}, bf16[128,512]{1,0:T(8,128)(2,1)}, u32[]{:S(2)}) copy-start(bf16[128,512]{1,0:T(8,128)(2,1)} %param.31) | copy-start | bytes 393220
  116.1 29.0 %copy-start.20 = (pred[384,128]{1,0:T(8,128)(4,1)S(1)}, pred[384,128]{1,0:T(8,128)(4,1)}, u32[]{:S(2)}) copy-start(pred[384,128]{1,0:T(8,128)(4,1)} %copy-done.19) | copy-start | bytes 147460
  116.1 28.6 %all-to-all-start.2 = ((bf16[8,2,12288]{2,1,0:T(2,128)(2,1)}), bf16[8,2,12288]{2,1,0:T(2,128)(2,1)S(1)}, u32[]{:S(2)}, u32[]{:S(2)}) async-start(bf16[8,2,12288]{2,1,0:T(2,128)(2,1)} %reshape.320), calls=%async_computation.3 | async-start | bytes 786432 | tf_op jit(solution)/shard_map/all_to_all | solution.py:218
  121.7 124.0 %all-gather.14.cloned.1.call-start = ((), (), s32[]{:S(2)}) async-start(), calls=%async_computation.10 | async-start | bytes 2359296 | tf_op jit(solution)/shard_map/all_gather | solution.py:21
  153.3 13.3 %copy-start.30 = (f32[128]{0:T(128)}, f32[128]{0:T(128)S(1)}, u32[]{:S(2)}) copy-start(f32[128]{0:T(128)S(1)} %broadcast_multiply_fusion) | copy-start | bytes 1540
  171.6 22.1 %copy-start.16 = (bf16[128,512]{1,0:T(8,128)(2,1)S(1)}, bf16[128,512]{1,0:T(8,128)(2,1)}, u32[]{:S(2)}) copy-start(bf16[128,512]{1,0:T(8,128)(2,1)} %param.32) | copy-start | bytes 393220
  172.3 23.5 %copy-start.25 = (bf16[128,1024]{1,0:T(8,128)(2,1)S(1)}, bf16[128,1024]{1,0:T(8,128)(2,1)}, u32[]{:S(2)}) copy-start(bf16[128,1024]{1,0:T(8,128)(2,1)} %param.30) | copy-start | bytes 786436
  172.4 138.4 %reduce-scatter.5.cloned.1.call-start = ((), (), s32[]{:S(2)}) async-start(), calls=%async_computation.8 | async-start | bytes 4718592 | tf_op jit(solution)/shard_map/reduce_scatter | solution.py:234
  173.6 26.7 %copy-start.5 = (bf16[4,128,256]{2,1,0:T(8,128)(2,1)}, bf16[4,128,256]{2,1,0:T(8,128)(2,1)S(1)}, u32[]{:S(2)}) copy-start(bf16[4,128,256]{2,1,0:T(8,128)(2,1)S(1)} %copy.213) | copy-start | bytes 786436
  222.8 15.1 %copy-start.8 = (f32[2,4,128,256]{3,2,1,0:T(8,128)S(1)}, f32[2,4,128,256]{3,2,1,0:T(8,128)}, u32[]{:S(2)}) copy-start(f32[2,4,128,256]{3,2,1,0:T(8,128)} %copy-done.7) | copy-start | bytes 3145732
  239.4 19.2 %copy-start.15 = (f32[16,4,8,128]{3,2,1,0:T(8,128)S(1)}, f32[16,4,8,128]{3,2,1,0:T(8,128)}, u32[]{:S(2)}) copy-start(f32[16,4,8,128]{3,2,1,0:T(8,128)} %multiply_bitcast_fusion) | copy-start | bytes 786436
  245.7 12.9 %copy-start.4 = (f32[2,4,128,256]{3,2,1,0:T(8,128)S(1)}, f32[2,4,128,256]{3,2,1,0:T(8,128)}, u32[]{:S(2)}) copy-start(f32[2,4,128,256]{3,2,1,0:T(8,128)} %get-tuple-element.225) | copy-start | bytes 3145732
  245.7 12.9 %copy-start.14 = (f32[16,4,8,128]{3,2,1,0:T(8,128)S(1)}, f32[16,4,8,128]{3,2,1,0:T(8,128)}, u32[]{:S(2)}) copy-start(f32[16,4,8,128]{3,2,1,0:T(8,128)} %convert_bitcast_fusion) | copy-start | bytes 786436
  245.7 12.9 %copy-start.27 = (f32[4,2,128]{2,0,1:T(4,128)S(1)}, f32[4,2,128]{2,0,1:T(4,128)}, u32[]{:S(2)}) copy-start(f32[4,2,128]{2,0,1:T(4,128)} %copy.222) | copy-start | bytes 12292
  263.7 49.1 %copy-start.1 = (bf16[1,2048,512]{2,1,0:T(8,128)(2,1)S(1)}, bf16[1,2048,512]{2,1,0:T(8,128)(2,1)}, u32[]{:S(2)}) copy-start(bf16[1,2048,512]{2,1,0:T(8,128)(2,1)} %param.26) | copy-start | bytes 6291460
  (20 other events, 63.7 us)
Sparse Core Ops, SparseCore 0:
  34.4 18.3 all-gather.7
  54.3 19.6 all-gather.9
  81.8 27.9 reduce-scatter.2
Sparse Core Ops, SparseCore 1:
  84.3 79.1 all-gather.11
  172.4 47.9 all-gather.13
  223.9 86.8 reduce-scatter.4
where the time goes:
time: 321 us; the launch traced here: 320 us
  waiting for transfers between devices  120 us (37%)
  blocking collectives  60.6 us (19%)
  other arithmetic  60 us (19%)
  matrix products  42 us (13%)
  between operations  16.1 us (5%)
  local copies, waits for them, and re-layouts  15.2 us (5%)
  starting transfers between devices  5.89 us (2%)
    reduce_scatter x1, waiting for transfers between devices, on_device(): lax.psum_scatter(lax.dot_general(resid_cols, mixed, (((0,), (0,)), ((), (...  42.4 us
    reduce_scatter x1, waiting for transfers between devices, on_device(): lax.psum_scatter(partial_short, 'tp', scatter_dimension=2, tiled=True)  27.6 us
    all_to_all x1, waiting for transfers between devices, on_device(): lax.all_to_all(summed, 'sp', split_axis=1, concat_axis=0, tiled=True)  21.2 us
    all_gather x1, blocking collectives, entering(): lax.all_gather(a.astype(kind), axis)  19.4 us
    all_to_all x1, blocking collectives, on_device(): lax.all_to_all(rows_in.reshape(experts, capacity, -1), 'sp', split_axis=0...  19.2 us
    all_gather x1, waiting for transfers between devices, on_device(): lax.all_gather(arrived[1], 'tp', axis=2, tiled=True)  15.3 us
    dot_general x1, other arithmetic, span_backward(): jnp.einsum('nts,nsd,ntsd->ntd', grad_scores, key_blk, decays, precision=h...  15.1 us
    all_to_all x1, blocking collectives, on_device(): lax.all_to_all(rows_cot.astype(jnp.bfloat16).reshape(experts, capacity, -...  15.1 us
  transfers between devices with their start and end apart: 7, of which 6 were waited for; matrix products, arithmetic and copies ran while one was open for 28% of the time, Pallas kernels for 0%

commit v1 on v0

v1 whole, which is shorter than its diff:
```python
import jax
import jax.numpy as jnp
from jax import lax
from jax.experimental import pallas as pl
from jax.experimental.pallas import tpu as pltpu
from jax.sharding import PartitionSpec as P

KEY_CHANNELS = 128
DV = 256
TOP = 2


epsilon = 1e-06
highest = lax.Precision.HIGHEST


SIDE = 16


def triangle(length, upper):
    rows = lax.broadcasted_iota(jnp.int32, (length, length), 0)
    cols = lax.broadcasted_iota(jnp.int32, (length, length), 1)
    return rows <= cols if upper else rows >= cols


def dot(a, b, ca, cb, precision=None):
    return lax.dot_general(
        a, b, (((ca,), (cb,)), ((), ())), preferred_element_type=jnp.float32, precision=precision
    )


def short(values):
    return values.astype(jnp.bfloat16)


def summary_kernel(resid_ref, proj_ref, query_ref, decay_ref, grad_ref, cum_ref, out_ref):
    length = query_ref.shape[0]
    grad = short(dot(resid_ref[...], proj_ref[...], 1, 0))
    grad_ref[...] = grad
    ones = triangle(length, False).astype(jnp.float32)
    cum = dot(ones, decay_ref[...], 1, 0, highest)
    cum_ref[...] = cum
    query = query_ref[...].astype(jnp.float32) * KEY_CHANNELS ** (-0.5)
    out_ref[0, 0:KEY_CHANNELS, :] = short(dot(short(query * jnp.exp(cum)), grad, 0, 0))
    total = jnp.exp(cum[length - 1 : length, :])
    upper = short(total)
    lower = short(total - upper.astype(jnp.float32))
    both = jnp.concatenate([upper.astype(jnp.float32), lower.astype(jnp.float32)], axis=1)
    out_ref[0, KEY_CHANNELS : KEY_CHANNELS + SIDE, :] = short(
        jnp.broadcast_to(both, (SIDE, both.shape[1]))
    )


def gradient_kernel(
    me_ref, all_ref, grad_ref, query_ref, key_ref, value_ref, cum_ref, state_ref,
    out_query, out_key, out_value, out_log,
):
    count = all_ref.shape[0]
    length = query_ref.shape[0]
    me = me_ref[0]
    sides = all_ref[:, 0, KEY_CHANNELS : KEY_CHANNELS + SIDE, :].astype(jnp.float32)
    sides = sides[:, 0, :]
    factors = (sides[:, :KEY_CHANNELS] + sides[:, KEY_CHANNELS : 2 * KEY_CHANNELS]).T
    exit_cot = jnp.zeros((KEY_CHANNELS, DV), jnp.float32)
    for j in range(count - 1, 0, -1):
        later = factors[:, j : j + 1] * exit_cot + all_ref[j, 0, 0:KEY_CHANNELS, :].astype(
            jnp.float32
        )
        exit_cot = jnp.where(j > me, later, exit_cot)
    exit_short = short(exit_cot)
    query_scale = KEY_CHANNELS ** (-0.5)
    cum = cum_ref[...]
    last = cum[length - 1 : length, :]
    middle = cum[length // 2 - 1 : length // 2, :]
    query = query_ref[...].astype(jnp.float32) * query_scale
    key = key_ref[...].astype(jnp.float32)
    grad = grad_ref[...]
    value = value_ref[...]
    state = state_ref[0, 0]
    rise = jnp.exp(cum - middle)
    fall = jnp.exp(middle - cum)
    to_end = jnp.exp(last - cum)
    causal = triangle(length, False)
    query_part = short(query * rise)
    key_part = short(key * fall)
    scores = short(jnp.where(causal, dot(query_part, key_part, 1, 1), 0.0))
    grad_scores = short(jnp.where(causal, dot(grad, value, 1, 1), 0.0))
    grad_query = rise * dot(grad_scores, key_part, 1, 0)
    grad_query = grad_query + jnp.exp(cum) * dot(grad, short(state), 1, 1)
    from_exit = dot(value, exit_short, 1, 1)
    key_end = key * to_end
    grad_key = fall * dot(grad_scores, query_part, 0, 0) + to_end * from_exit
    grad_value = dot(scores, grad, 0, 0) + dot(short(key_end), exit_short, 1, 0)
    product = dot(jnp.ones((8, DV), jnp.float32), state * exit_cot, 1, 1, highest)[0:1, :]
    tail = jnp.exp(last) * product + jnp.sum(key_end * from_exit, axis=0, keepdims=True)
    ones = triangle(length, True).astype(jnp.float32)
    out_log[...] = dot(ones, query * grad_query - key * grad_key, 1, 0, highest) + tail
    out_query[...] = short(grad_query * query_scale)
    out_key[...] = short(grad_key)
    out_value[...] = short(grad_value)


def on_device(
    resid,
    norm_gain,
    cotangent,
    route_ids,
    route_weight,
    expert_gate,
    expert_up,
    expert_down,
    out_proj,
    mixed,
    query,
    key,
    value,
    log_decay,
    span_state,
):
    tokens_here = resid.shape[0]
    model_width = resid.shape[1]
    sp_count = lax.axis_size("sp")
    tp_count = lax.axis_size("tp")
    experts = sp_count * expert_gate.shape[0]
    capacity = 3 * tokens_here // experts
    resid_f = resid.astype(jnp.float32)
    inverse_rms = lax.rsqrt(jnp.mean(resid_f * resid_f, axis=1, keepdims=True) + epsilon)
    unit_rows = resid_f * inverse_rms
    normed = (unit_rows * norm_gain).astype(jnp.bfloat16)
    pair_expert = route_ids.reshape(-1)
    onehot = (pair_expert[:, None] == jnp.arange(experts, dtype=jnp.int32)[None, :]).astype(
        jnp.int32
    )
    slot_rank = jnp.sum((jnp.cumsum(onehot, axis=0) - onehot) * onehot, axis=1)
    slot_of = pair_expert * capacity + slot_rank
    slot_pairs = slot_of[None, :] == jnp.arange(experts * capacity, dtype=jnp.int32)[:, None]
    slot_tokens = jnp.any(slot_pairs.reshape(experts * capacity, tokens_here, TOP), axis=2).astype(
        jnp.bfloat16
    )
    slot_weight = jnp.sum(jnp.where(slot_pairs, route_weight.reshape(1, -1), 0.0), axis=1)
    column_share = model_width // tp_count
    offset = lax.axis_index("tp") * column_share
    rows_in = jnp.dot(
        slot_tokens,
        lax.dynamic_slice_in_dim(normed, offset, column_share, 1),
        preferred_element_type=jnp.float32,
    ).astype(jnp.bfloat16)
    rows_cot = (
        jnp.dot(
            slot_tokens,
            lax.dynamic_slice_in_dim(cotangent, offset, column_share, 1),
            preferred_element_type=jnp.float32,
        )
        * slot_weight[:, None]
    )
    arrived = tuple(
        lax.all_to_all(
            rows.reshape(experts, capacity, -1), "sp", split_axis=0, concat_axis=0, tiled=True
        ).reshape(1, experts * capacity, -1)
        for rows in (rows_in, rows_cot.astype(jnp.bfloat16))
    )
    mixed_all = lax.all_gather(mixed, "sp", axis=0, tiled=True)
    expert_in, expert_cot = (
        lax.all_gather(arrived[0], "tp", axis=2, tiled=True),
        lax.all_gather(arrived[1], "tp", axis=2, tiled=True),
    )
    gate_pre = jnp.einsum(
        "erd,edf->erf", expert_in, expert_gate, preferred_element_type=jnp.float32
    )
    up_pre = jnp.einsum("erd,edf->erf", expert_in, expert_up, preferred_element_type=jnp.float32)
    gate_sig = jax.nn.sigmoid(gate_pre)
    hidden = (gate_pre * gate_sig * up_pre).astype(jnp.bfloat16)
    grad_hidden = jnp.einsum(
        "erd,efd->erf", expert_cot, expert_down, preferred_element_type=jnp.float32
    )
    grad_up_act = (grad_hidden * gate_pre * gate_sig).astype(jnp.bfloat16)
    grad_gate_act = (grad_hidden * up_pre * gate_sig * (1.0 + gate_pre * (1.0 - gate_sig))).astype(
        jnp.bfloat16
    )
    grad_down_w = jnp.einsum("erf,erd->efd", hidden, expert_cot, preferred_element_type=jnp.float32)
    grad_gate_w = jnp.einsum(
        "erd,erf->edf", expert_in, grad_gate_act, preferred_element_type=jnp.float32
    )
    grad_up_w = jnp.einsum(
        "erd,erf->edf", expert_in, grad_up_act, preferred_element_type=jnp.float32
    )
    partial_value = jnp.einsum(
        "erf,edf->erd", grad_gate_act, expert_gate, preferred_element_type=jnp.float32
    )
    partial_value = partial_value + jnp.einsum(
        "erf,edf->erd", grad_up_act, expert_up, preferred_element_type=jnp.float32
    )
    partial_short = partial_value.astype(jnp.bfloat16)
    summed = (
        lax.psum_scatter(partial_short, "tp", scatter_dimension=2, tiled=True)
        .astype(jnp.float32)
        .astype(jnp.bfloat16)
    )
    returned = lax.all_to_all(
        summed.reshape(experts, capacity, -1), "sp", split_axis=0, concat_axis=0, tiled=True
    )
    flat_rows = returned.reshape(experts * capacity, -1)
    grad_normed = lax.all_gather(
        lax.dot_general(
            slot_tokens, flat_rows, (((0,), (0,)), ((), ())), preferred_element_type=jnp.float32
        ).astype(jnp.bfloat16),
        "tp",
        axis=1,
        tiled=True,
    ).astype(jnp.float32)
    scaled = grad_normed * norm_gain
    grad_resid = cotangent.astype(jnp.float32) + inverse_rms * (
        scaled - unit_rows * jnp.mean(scaled * unit_rows, axis=1, keepdims=True)
    )
    grad_resid = grad_resid.astype(jnp.bfloat16)
    resid_all = lax.all_to_all(grad_resid, "sp", split_axis=1, concat_axis=0, tiled=True)
    proj_all = lax.all_gather(out_proj, "sp", axis=0, tiled=True)
    heads = query.shape[1] // KEY_CHANNELS
    narrow = pl.BlockSpec((tokens_here, KEY_CHANNELS), lambda h: (0, h))
    wide = pl.BlockSpec((tokens_here, DV), lambda h: (0, h))
    rows_kept = KEY_CHANNELS + SIDE
    grad_mixed, cum, own = pl.pallas_call(
        summary_kernel,
        grid=(heads,),
        in_specs=[
            pl.BlockSpec((tokens_here, model_width), lambda h: (0, 0)),
            pl.BlockSpec((model_width, DV), lambda h: (0, h)),
            narrow,
            narrow,
        ],
        out_specs=[wide, narrow, pl.BlockSpec((1, rows_kept, DV), lambda h: (h, 0, 0))],
        out_shape=[
            jax.ShapeDtypeStruct((tokens_here, heads * DV), jnp.bfloat16),
            jax.ShapeDtypeStruct((tokens_here, heads * KEY_CHANNELS), jnp.float32),
            jax.ShapeDtypeStruct((heads, rows_kept, DV), jnp.bfloat16),
        ],
        cost_estimate=pl.CostEstimate(
            flops=2 * tokens_here * heads * DV * (model_width + 2 * KEY_CHANNELS),
            bytes_accessed=2 * model_width * heads * DV + 8 * tokens_here * heads * DV,
            transcendentals=tokens_here * heads * KEY_CHANNELS,
        ),
        name="summary",
    )(grad_resid, proj_all, query, log_decay)
    gathered = lax.all_gather(own, "sp")
    me = lax.axis_index("sp").reshape(1).astype(jnp.int32)
    grad_query, grad_key, grad_value, grad_log_decay = pl.pallas_call(
        gradient_kernel,
        grid=(heads,),
        in_specs=[
            pl.BlockSpec(memory_space=pltpu.SMEM),
            pl.BlockSpec((sp_count, 1, rows_kept, DV), lambda h: (0, h, 0, 0)),
            wide,
            narrow,
            narrow,
            wide,
            narrow,
            pl.BlockSpec((1, 1, KEY_CHANNELS, DV), lambda h: (0, h, 0, 0)),
        ],
        out_specs=[narrow, narrow, wide, narrow],
        out_shape=[
            jax.ShapeDtypeStruct(query.shape, jnp.bfloat16),
            jax.ShapeDtypeStruct(key.shape, jnp.bfloat16),
            jax.ShapeDtypeStruct(value.shape, jnp.bfloat16),
            jax.ShapeDtypeStruct(log_decay.shape, jnp.float32),
        ],
        cost_estimate=pl.CostEstimate(
            flops=40 * tokens_here * heads * DV * KEY_CHANNELS,
            bytes_accessed=2 * sp_count * heads * rows_kept * DV + 24 * tokens_here * heads * DV,
            transcendentals=5 * tokens_here * heads * KEY_CHANNELS,
        ),
        name="gradients",
    )(me, gathered, grad_mixed, query, key, value, cum, span_state)
    grad_out_proj = lax.dot_general(
        resid_all, mixed_all, (((0,), (0,)), ((), ())), preferred_element_type=jnp.float32
    )
    return (
        grad_gate_w.astype(jnp.bfloat16),
        grad_up_w.astype(jnp.bfloat16),
        grad_down_w.astype(jnp.bfloat16),
        grad_out_proj,
        grad_query,
        grad_key,
        grad_value,
        grad_log_decay,
    )


def solution(mesh):
    return jax.shard_map(
        on_device,
        mesh=mesh,
        in_specs=(
            P("sp", None),
            P(),
            P("sp", None),
            P("sp", None),
            P("sp", None),
            P("sp", None, "tp"),
            P("sp", None, "tp"),
            P("sp", "tp", None),
            P("sp", "tp"),
            P("sp", "tp"),
            P("sp", "tp"),
            P("sp", "tp"),
            P("sp", "tp"),
            P("sp", "tp"),
            P("sp", "tp", None, None),
        ),
        out_specs=(
            P("sp", None, "tp"),
            P("sp", None, "tp"),
            P("sp", "tp", None),
            P("sp", "tp"),
            P("sp", "tp"),
            P("sp", "tp"),
            P("sp", "tp"),
            P("sp", "tp"),
        ),
        check_vma=False,
    )
```

time: 321 us -> 283 us (0.88)
  other arithmetic: 60 us -> 5.59 us
  waiting for transfers between devices: 120 us -> 149 us
  matrix products: 42 us -> 25.5 us
  local copies, waits for them, and re-layouts: 15.2 us -> 3.69 us
  Pallas kernels: 0 us -> 10.6 us
  blocking collectives: 60.6 us -> 67.6 us
    all_gather x2 -> x3, waiting for transfers between devices: 10.2 us -> 103 us  [the longest x1 49.1 us: on_device(): gathered = lax.all_gather(own, 'sp')]
    reduce_scatter x1 -> x0, waiting for transfers between devices: 42.4 us -> none  [on_device(): lax.psum_scatter(lax.dot_general(resid_cols, mixed, (((0,), (0,)), ((), (...]
    dot_general x3 -> x0, other arithmetic: 30.8 us -> none  [the longest x1 15.1 us: span_backward(): jnp.einsum('nts,nsd,ntsd->ntd', grad_scores, key_blk, decays, precision=h...]
    all_to_all x2 -> x3, blocking collectives: 34.3 us -> 61.1 us  [the longest x2 34.3 us: on_device(): lax.all_to_all(rows.reshape(experts, capacity, -1), 'sp', split_axis=0, c...]
    all_to_all x1, waiting for transfers between devices: 21.2 us -> 0.01 us  [on_device(): lax.all_to_all(grad_resid, 'sp', split_axis=1, concat_axis=0, tiled=True)]
    all_gather x1 -> x0, blocking collectives: 19.4 us -> none  [entering(): lax.all_gather(a.astype(kind), axis)]
    dot_general x9 -> x1, matrix products: 17.6 us -> 3.29 us  [on_device(): lax.dot_general(resid_all, mixed_all, (((0,), (0,)), ((), ())), preferred...]
    pallas_call x0 -> x2, Pallas kernels: none -> 10.6 us  [the longest x1 5.55 us: on_device(): pl.pallas_call(gradient_kernel, grid=(heads,), in_specs=[pl.BlockSpec(mem...]
  transfers between devices with their start and end apart: 7 -> 7, of which waited for: 6 -> 6; matrix products, arithmetic and copies ran while one was open for 28% -> 8% of each run, Pallas kernels for 0% -> 2%
where the time goes in v1:
time: 283 us; the launch traced here: 282 us
  waiting for transfers between devices  149 us (53%)
  blocking collectives  67.6 us (24%)
  matrix products  25.5 us (9%)
  between operations  15.7 us (6%)
  Pallas kernels  10.6 us (4%)
  other arithmetic  5.59 us (2%)
  starting transfers between devices  3.92 us (1%)
  local copies, waits for them, and re-layouts  3.69 us (1%)
    all_gather x1, waiting for transfers between devices, on_device(): gathered = lax.all_gather(own, 'sp')  49.1 us
    all_gather x1, waiting for transfers between devices, on_device(): mixed_all = lax.all_gather(mixed, 'sp', axis=0, tiled=True)  37.5 us
    all_to_all x2, blocking collectives, on_device(): lax.all_to_all(rows.reshape(experts, capacity, -1), 'sp', split_axis=0, c...  34.3 us
    reduce_scatter x1, waiting for transfers between devices, on_device(): lax.psum_scatter(partial_short, 'tp', scatter_dimension=2, tiled=True)  26.9 us
    all_to_all x1, blocking collectives, on_device(): lax.all_to_all(summed.reshape(experts, capacity, -1), 'sp', split_axis=0,...  26.8 us
    all_gather x1, waiting for transfers between devices, on_device(): lax.all_gather(arrived[1], 'tp', axis=2, tiled=True)  16.8 us
    all_gather x1, waiting for transfers between devices, on_device(): proj_all = lax.all_gather(out_proj, 'sp', axis=0, tiled=True)  16.2 us
    all_gather x1, blocking collectives, on_device(): lax.all_gather(lax.dot_general(slot_tokens, flat_rows, (((0,), (0,)), (()...  6.5 us
  transfers between devices with their start and end apart: 7, of which 6 were waited for; matrix products, arithmetic and copies ran while one was open for 8% of the time, Pallas kernels for 2%

profile of v1, /device:TPU:0, one launch (start us, length us, event | category | flops | bytes accessed | tf_op | source)
XLA Modules:
  0.0 282.0 jit_solution(2798796686445430926)
XLA Ops:
  11.2 1.2 fusion.20
  12.4 1.2 convert_multiply_fusion
  14.0 19.2 %all_to_all.34 = bf16[8,48,512]{2,1,0:T(8,128)(2,1)} all-to-all(bf16[8,48,512]{2,1,0:T(8,128)(2,1)S(1)} %bitcast.77), channel_id=1, replica_groups=mesh['sp'=8,'tp'=4] {'sp'}, dimensions={0} | all-to-all | bytes 786432 | tf_op jit(solution)/shard_map/all_to_all | solution.py:157
  34.9 15.1 %all_to_all.35 = bf16[8,48,512]{2,1,0:T(8,128)(2,1)} all-to-all(bf16[8,48,512]{2,1,0:T(8,128)(2,1)S(1)} %bitcast.79), channel_id=1, replica_groups=mesh['sp'=8,'tp'=4] {'sp'}, dimensions={0} | all-to-all | bytes 786432 | tf_op jit(solution)/shard_map/all_to_all | solution.py:157
  50.0 1.7 all-gather.7.cloned.1.call-done
  51.8 2.5 fusion.6
  54.3 1.9 fusion.9
  56.2 16.8 %all-gather.9.cloned.1.call-done = bf16[1,384,2048]{2,1,0:T(8,128)(2,1)} async-done(((bf16[1,384,512]{2,1,0:T(8,128)(2,1)}), bf16[1,384,2048]{2,1,0:T(8,128)(2,1)}) %all-gather.9.cloned.1.call-update) | async-done | bytes 1572880 | tf_op jit(solution)/shard_map/all_gather | solution.py:165
  73.0 3.5 %multiply_convert_fusion.1 = (bf16[384,512]{1,0:T(8,128)(2,1)S(1)}, bf16[384,512]{1,0:T(8,128)(2,1)S(1)}) fusion(f32[384,512]{1,0:T(8,128)S(1)} %fusion.6, f32[384,512]{1,0:T(8,128)} %fusion.9, bf16[1,512,2048]{2,1,0:T(8,128)(2,1)} %param.22, bf16[1,384,2048]{2,1,0:T(8,128)(2,1)} %all-gather.9.cloned.1.call-done), kind=kOutput, calls=%fused_computation.34 | convolution fusion | flops 807862272 | bytes 6029312 | tf_op jit(solution)/shard_map/erd,efd->erf/dot_general | solution.py:173
  78.3 2.2 fusion.3
  81.8 26.9 %reduce-scatter.2.cloned.1.call-done = bf16[1,384,512]{2,1,0:T(8,128)(2,1)} async-done(((bf16[1,384,2048]{2,1,0:T(8,128)(2,1)}), bf16[1,384,512]{2,1,0:T(8,128)(2,1)}) %reduce-scatter.2.cloned.1.call-update) | async-done | bytes 393232 | tf_op jit(solution)/shard_map/reduce_scatter | solution.py:195
  108.6 26.8 %all_to_all.36 = bf16[8,48,512]{2,1,0:T(8,128)(2,1)S(1)} all-to-all(bf16[8,48,512]{2,1,0:T(8,128)(2,1)} %bitcast.80), channel_id=1, replica_groups=mesh['sp'=8,'tp'=4] {'sp'}, dimensions={0} | all-to-all | bytes 786432 | tf_op jit(solution)/shard_map/all_to_all | solution.py:199
  135.7 6.5 %all_gather.23 = bf16[128,2048]{1,0:T(8,128)(2,1)S(1)} all-gather(bf16[128,512]{1,0:T(8,128)(2,1)S(1)} %convolution_convert_fusion.4), channel_id=1, replica_groups=mesh['sp'=8,'tp'=4] {'tp'}, dimensions={1}, use_global_device_ids=true | all-gather | bytes 655360 | tf_op jit(solution)/shard_map/all_gather | solution.py:203
  142.6 1.2 add_convert_fusion.1.resid_ref
  143.8 16.2 %all-gather.13.cloned.1.call-done.proj_ref = bf16[2048,1024]{1,0:T(8,128)(2,1)} async-done(((bf16[256,1024]{1,0:T(8,128)(2,1)}), bf16[2048,1024]{1,0:T(8,128)(2,1)}) %all-gather.13.cloned.1.call-update) | async-done | bytes 4194320 | tf_op jit(solution)/shard_map/all_gather | solution.py:217
  160.0 5.1 %summary.1 = (bf16[128,1024]{1,0:T(8,128)(2,1)}, f32[128,512]{1,0:T(8,128)}, bf16[4,144,256]{2,1,0:T(8,128)(2,1)}) custom-call(bf16[128,2048]{1,0:T(8,128)(2,1)} %add_convert_fusion.1.resid_ref, bf16[2048,1024]{1,0:T(8,128)(2,1)} %all-gather.13.cloned.1.call-done.proj_ref, bf16[128,512]{1,0:T(8,128)(2,1)} %query_ref.3, f32[128,512]{1,0:T(8,128)} %decay_ref.1), custom_call_target="tpu_custom_call" | custom-call | flops 603979776 | bytes 5242880 | tf_op jit(solution)/shard_map/summary/pallas_call | solution.py:222
  165.9 3.7 %all-to-all-start.3 = ((bf16[128,8,256]{2,0,1:T(8,128)(2,1)}), bf16[128,8,256]{2,0,1:T(8,128)(2,1)S(1)}, u32[]{:S(2)}, u32[]{:S(2)}) async-start(bf16[128,8,256]{2,0,1:T(8,128)(2,1)} %bitcast.71), calls=%async_computation.4 | async-start | bytes 1048576 | tf_op jit(solution)/shard_map/all_to_all | solution.py:216
  169.7 4.2 %fusion.1 = bf16[1,2048,512]{2,1,0:T(8,128)(2,1)} fusion(bf16[384,512]{1,0:T(8,128)(2,1)S(1)} %copy-done.7, bf16[1,384,2048]{2,1,0:T(8,128)(2,1)} %all-gather.7.cloned.1.call-done), kind=kOutput, calls=%fused_computation.5 | convolution fusion | flops 806354944 | bytes 4063232 | tf_op jit(solution)/shard_map/erd,erf->edf/dot_general | solution.py:184
  173.9 2.6 fusion
  176.5 2.7 fusion.2
  179.2 37.5 %all-gather.11.cloned.1.call-done = bf16[1024,1024]{1,0:T(8,128)(2,1)} async-done(((bf16[128,1024]{1,0:T(8,128)(2,1)}), bf16[1024,1024]{1,0:T(8,128)(2,1)}) %all-gather.11.cloned.1.call-update) | async-done | bytes 2097168 | tf_op jit(solution)/shard_map/all_gather | solution.py:162
  216.7 3.3 %fusion.33 = f32[256,1024]{1,0:T(8,128)} fusion(bf16[1024,256]{1,0:T(8,128)(2,1)S(1)} %bitcast.74, bf16[1024,1024]{1,0:T(8,128)(2,1)} %all-gather.11.cloned.1.call-done), kind=kOutput, calls=%fused_computation.61 | convolution fusion | flops 536870912 | bytes 3670016 | tf_op jit(solution)/shard_map/dot_general | solution.py:273
  220.0 49.1 %all-gather.15.cloned.1.call-done = bf16[32,144,256]{2,1,0:T(8,128)(2,1)} async-done(((bf16[4,144,256]{2,1,0:T(8,128)(2,1)}), bf16[32,144,256]{2,1,0:T(8,128)(2,1)}) %all-gather.15.cloned.1.call-update) | async-done | bytes 2359312 | tf_op jit(solution)/shard_map/all_gather | solution.py:244
  269.1 5.6 %gradients.1 = (bf16[128,512]{1,0:T(8,128)(2,1)}, bf16[128,512]{1,0:T(8,128)(2,1)}, bf16[128,1024]{1,0:T(8,128)(2,1)}, f32[128,512]{1,0:T(8,128)}) custom-call(s32[1]{0:T(128)} %bitcast.19.me_ref, bf16[8,4,144,256]{3,2,1,0:T(8,128)(2,1)} %bitcast.73, bf16[128,1024]{1,0:T(8,128)(2,1)} %get-tuple-element.16.grad_ref, bf16[128,512]{1,0:T(8,128)(2,1)} %query_ref.3, ...), custom_call_target="tpu_custom_call" | custom-call | flops 671088640 | bytes 5505024 | tf_op jit(solution)/shard_map/gradients/pallas_call | solution.py:246
  (75 shorter events, 9.8 us)
Async XLA Ops:
  8.0 43.7 %copy-start = (bf16[1,2048,512]{2,1,0:T(8,128)(2,1)S(1)}, bf16[1,2048,512]{2,1,0:T(8,128)(2,1)}, u32[]{:S(2)}) copy-start(bf16[1,2048,512]{2,1,0:T(8,128)(2,1)} %param.20) | copy-start | bytes 6291460
  8.0 5.6 %copy-start.10 = (f32[2048]{0:T(1024)S(1)}, f32[2048]{0:T(1024)}, u32[]{:S(2)}) copy-start(f32[2048]{0:T(1024)} %param.16) | copy-start | bytes 24580
  8.0 43.7 %all-gather.7.cloned.1.call-start = ((), (), s32[]{:S(2)}) async-start(), calls=%async_computation.5 | async-start | bytes 1966080 | tf_op jit(solution)/shard_map/all_gather | solution.py:164
  10.1 23.2 %copy-start.11 = (f32[128,2]{0,1:T(2,128)S(1)}, f32[128,2]{0,1:T(2,128)}, u32[]{:S(2)}) copy-start(f32[128,2]{0,1:T(2,128)} %param.19) | copy-start | bytes 3076
  33.2 39.7 %all-gather.9.cloned.1.call-start = ((), (), s32[]{:S(2)}) async-start(), calls=%async_computation.6 | async-start | bytes 1966080 | tf_op jit(solution)/shard_map/all_gather | solution.py:165
  50.0 58.7 %reduce-scatter.2.cloned.1.call-start = ((), (), s32[]{:S(2)}) async-start(), calls=%async_computation.7 | async-start | bytes 1966080 | tf_op jit(solution)/shard_map/reduce_scatter | solution.py:195
  51.7 2.5 copy-start.3
  51.7 2.5 copy-start.12
  54.3 18.7 %copy-start.15 = (f32[384,512]{1,0:T(8,128)}, f32[384,512]{1,0:T(8,128)S(1)}, u32[]{:S(2)}) copy-start(f32[384,512]{1,0:T(8,128)S(1)} %fusion.6) | copy-start | bytes 2359300
  76.4 1.1 copy-start.8
  76.5 1.9 copy-start.4
  80.5 61.7 %copy-start.1 = (bf16[128,2048]{1,0:T(8,128)(2,1)S(1)}, bf16[128,2048]{1,0:T(8,128)(2,1)}, u32[]{:S(2)}) copy-start(bf16[128,2048]{1,0:T(8,128)(2,1)} %param.15) | copy-start | bytes 1572868
  80.5 62.0 %copy-start.5 = (bf16[128,2048]{1,0:T(8,128)(2,1)S(1)}, bf16[128,2048]{1,0:T(8,128)(2,1)}, u32[]{:S(2)}) copy-start(bf16[128,2048]{1,0:T(8,128)(2,1)} %param.17) | copy-start | bytes 1572868
  80.5 79.4 %all-gather.13.cloned.1.call-start = ((), (), s32[]{:S(2)}) async-start(), calls=%async_computation.9 | async-start | bytes 4718592 | tf_op jit(solution)/shard_map/all_gather | solution.py:217
  81.1 135.6 %all-gather.11.cloned.1.call-start = ((), (), s32[]{:S(2)}) async-start(), calls=%async_computation.8 | async-start | bytes 2359296 | tf_op jit(solution)/shard_map/all_gather | solution.py:162
  81.7 187.4 %all-gather.15.cloned.1.call-start = ((), (), s32[]{:S(2)}) async-start(), calls=%async_computation.10 | async-start | bytes 2654208 | tf_op jit(solution)/shard_map/all_gather | solution.py:244
  143.8 21.3 %copy-start.2 = (bf16[128,2048]{1,0:T(8,128)(2,1)S(1)}, bf16[128,2048]{1,0:T(8,128)(2,1)}, u32[]{:S(2)}) copy-start(bf16[128,2048]{1,0:T(8,128)(2,1)} %add_convert_fusion.1.resid_ref) | copy-start | bytes 1572868
  165.1 4.6 %copy-start.7 = (bf16[384,512]{1,0:T(8,128)(2,1)S(1)}, bf16[384,512]{1,0:T(8,128)(2,1)}, u32[]{:S(2)}) copy-start(bf16[384,512]{1,0:T(8,128)(2,1)} %copy-done.6) | copy-start | bytes 1179652
  165.9 50.8 %all-to-all-start.3 = ((bf16[128,8,256]{2,0,1:T(8,128)(2,1)}), bf16[128,8,256]{2,0,1:T(8,128)(2,1)S(1)}, u32[]{:S(2)}, u32[]{:S(2)}) async-start(bf16[128,8,256]{2,0,1:T(8,128)(2,1)} %bitcast.71), calls=%async_computation.4 | async-start | bytes 1048576 | tf_op jit(solution)/shard_map/all_to_all | solution.py:216
  169.6 4.2 %copy-start.9 = (bf16[384,512]{1,0:T(8,128)(2,1)S(1)}, bf16[384,512]{1,0:T(8,128)(2,1)}, u32[]{:S(2)}) copy-start(bf16[384,512]{1,0:T(8,128)(2,1)} %copy-done.8) | copy-start | bytes 1179652
  169.7 4.2 %copy-start.13 = (bf16[1,384,2048]{2,1,0:T(8,128)(2,1)S(1)}, bf16[1,384,2048]{2,1,0:T(8,128)(2,1)}, u32[]{:S(2)}) copy-start(bf16[1,384,2048]{2,1,0:T(8,128)(2,1)} %all-gather.7.cloned.1.call-done) | copy-start | bytes 4718596
  173.8 2.6 copy-start.14
  173.8 2.6 copy-start.16
  173.9 2.6 copy-start.17
  (1 other events, 1.1 us)
Sparse Core Ops, SparseCore 0:
  33.4 18.3 all-gather.6
  53.3 19.6 all-gather.8
  80.6 27.9 reduce-scatter.1
Sparse Core Ops, SparseCore 1:
  83.1 76.8 all-gather.12
  162.0 54.7 all-gather.10
  218.8 50.2 all-gather.14

commit v2 on v1

--- a/solution.py
+++ b/solution.py
@@ -2,7 +2,6 @@
 import jax.numpy as jnp
 from jax import lax
 from jax.experimental import pallas as pl
-from jax.experimental.pallas import tpu as pltpu
 from jax.sharding import PartitionSpec as P
 
 KEY_CHANNELS = 128
@@ -14,7 +13,7 @@
 highest = lax.Precision.HIGHEST
 
 
-SIDE = 16
+SIDE = 64
 
 
 def triangle(length, upper):
@@ -41,33 +40,21 @@
     cum = dot(ones, decay_ref[...], 1, 0, highest)
     cum_ref[...] = cum
     query = query_ref[...].astype(jnp.float32) * KEY_CHANNELS ** (-0.5)
-    out_ref[0, 0:KEY_CHANNELS, :] = short(dot(short(query * jnp.exp(cum)), grad, 0, 0))
-    total = jnp.exp(cum[length - 1 : length, :])
-    upper = short(total)
-    lower = short(total - upper.astype(jnp.float32))
-    both = jnp.concatenate([upper.astype(jnp.float32), lower.astype(jnp.float32)], axis=1)
-    out_ref[0, KEY_CHANNELS : KEY_CHANNELS + SIDE, :] = short(
-        jnp.broadcast_to(both, (SIDE, both.shape[1]))
-    )
+    out_ref[0, :, 0:DV] = short(dot(short(query * jnp.exp(cum)), grad, 0, 0))
+    fill = jnp.ones((length, 2 * SIDE), jnp.float32)
+    total = jnp.exp(dot(decay_ref[...], fill, 0, 0, highest))
+    upper = short(total).astype(jnp.float32)
+    lanes = lax.broadcasted_iota(jnp.int32, total.shape, 1)
+    out_ref[0, :, DV : DV + 2 * SIDE] = short(jnp.where(lanes < SIDE, upper, total - upper))
 
 
 def gradient_kernel(
-    me_ref, all_ref, grad_ref, query_ref, key_ref, value_ref, cum_ref, state_ref,
+    exit_ref, grad_ref, query_ref, key_ref, value_ref, cum_ref, state_ref,
     out_query, out_key, out_value, out_log,
 ):
-    count = all_ref.shape[0]
     length = query_ref.shape[0]
-    me = me_ref[0]
-    sides = all_ref[:, 0, KEY_CHANNELS : KEY_CHANNELS + SIDE, :].astype(jnp.float32)
-    sides = sides[:, 0, :]
-    factors = (sides[:, :KEY_CHANNELS] + sides[:, KEY_CHANNELS : 2 * KEY_CHANNELS]).T
-    exit_cot = jnp.zeros((KEY_CHANNELS, DV), jnp.float32)
-    for j in range(count - 1, 0, -1):
-        later = factors[:, j : j + 1] * exit_cot + all_ref[j, 0, 0:KEY_CHANNELS, :].astype(
-            jnp.float32
-        )
-        exit_cot = jnp.where(j > me, later, exit_cot)
-    exit_short = short(exit_cot)
+    exit_short = exit_ref[0]
+    exit_cot = exit_short.astype(jnp.float32)
     query_scale = KEY_CHANNELS ** (-0.5)
     cum = cum_ref[...]
     last = cum[length - 1 : length, :]
@@ -218,7 +205,7 @@
     heads = query.shape[1] // KEY_CHANNELS
     narrow = pl.BlockSpec((tokens_here, KEY_CHANNELS), lambda h: (0, h))
     wide = pl.BlockSpec((tokens_here, DV), lambda h: (0, h))
-    rows_kept = KEY_CHANNELS + SIDE
+    packed = DV + 2 * SIDE
     grad_mixed, cum, own = pl.pallas_call(
         summary_kernel,
         grid=(heads,),
@@ -228,11 +215,11 @@
             narrow,
             narrow,
         ],
-        out_specs=[wide, narrow, pl.BlockSpec((1, rows_kept, DV), lambda h: (h, 0, 0))],
+        out_specs=[wide, narrow, pl.BlockSpec((1, KEY_CHANNELS, packed), lambda h: (h, 0, 0))],
         out_shape=[
             jax.ShapeDtypeStruct((tokens_here, heads * DV), jnp.bfloat16),
             jax.ShapeDtypeStruct((tokens_here, heads * KEY_CHANNELS), jnp.float32),
-            jax.ShapeDtypeStruct((heads, rows_kept, DV), jnp.bfloat16),
+            jax.ShapeDtypeStruct((heads, KEY_CHANNELS, packed), jnp.bfloat16),
         ],
         cost_estimate=pl.CostEstimate(
             flops=2 * tokens_here * heads * DV * (model_width + 2 * KEY_CHANNELS),
@@ -241,14 +228,38 @@
         ),
         name="summary",
     )(grad_resid, proj_all, query, log_decay)
-    gathered = lax.all_gather(own, "sp")
-    me = lax.axis_index("sp").reshape(1).astype(jnp.int32)
+    share = KEY_CHANNELS // sp_count
+    own_rows = own.reshape(heads, sp_count, share, packed).transpose(1, 0, 2, 3)
+    spans = lax.all_to_all(
+        own_rows.reshape(sp_count, heads * share, packed),
+        "sp",
+        split_axis=0,
+        concat_axis=0,
+        tiled=True,
+    ).astype(jnp.float32)
+    running = jnp.zeros((heads * share, DV), jnp.float32)
+    exits = [running]
+    for span in range(sp_count - 1, 0, -1):
+        factor = spans[span, :, DV : DV + 1] + spans[span, :, DV + SIDE : DV + SIDE + 1]
+        running = spans[span, :, :DV] + factor * running
+        exits.append(running)
+    exit_rows = lax.all_to_all(
+        jnp.stack(exits[::-1]).astype(jnp.bfloat16),
+        "sp",
+        split_axis=0,
+        concat_axis=0,
+        tiled=True,
+    )
+    exit_all = (
+        exit_rows.reshape(sp_count, heads, share, DV)
+        .transpose(1, 0, 2, 3)
+        .reshape(heads, KEY_CHANNELS, DV)
+    )
     grad_query, grad_key, grad_value, grad_log_decay = pl.pallas_call(
         gradient_kernel,
         grid=(heads,),
         in_specs=[
-            pl.BlockSpec(memory_space=pltpu.SMEM),
-            pl.BlockSpec((sp_count, 1, rows_kept, DV), lambda h: (0, h, 0, 0)),
+            pl.BlockSpec((1, KEY_CHANNELS, DV), lambda h: (h, 0, 0)),
             wide,
             narrow,
             narrow,
@@ -265,11 +276,11 @@
         ],
         cost_estimate=pl.CostEstimate(
             flops=40 * tokens_here * heads * DV * KEY_CHANNELS,
-            bytes_accessed=2 * sp_count * heads * rows_kept * DV + 24 * tokens_here * heads * DV,
+            bytes_accessed=2 * heads * KEY_CHANNELS * DV + 24 * tokens_here * heads * DV,
             transcendentals=5 * tokens_here * heads * KEY_CHANNELS,
         ),
         name="gradients",
-    )(me, gathered, grad_mixed, query, key, value, cum, span_state)
+    )(exit_all, grad_mixed, query, key, value, cum, span_state)
     grad_out_proj = lax.dot_general(
         resid_all, mixed_all, (((0,), (0,)), ((), ())), preferred_element_type=jnp.float32
     )

time: 283 us -> 247 us (0.87)
  waiting for transfers between devices: 149 us -> 122 us
  blocking collectives: 67.6 us -> 40.8 us
  starting transfers between devices: 3.92 us -> 16.3 us
  local copies, waits for them, and re-layouts: 3.69 us -> 6.88 us
    all_gather x1 -> x0, waiting for transfers between devices: 49.1 us -> none  [on_device(): gathered = lax.all_gather(own, 'sp')]
    all_gather x1, waiting for transfers between devices: 37.5 us -> 0.01 us  [on_device(): mixed_all = lax.all_gather(mixed, 'sp', axis=0, tiled=True)]
    all_to_all x0 -> x3, waiting for transfers between devices: none -> 32.1 us  [the longest x1 20.6 us: on_device(): lax.all_to_all(summed.reshape(experts, capacity, -1), 'sp', split_axis=0,...]
    all_to_all x1, waiting for transfers between devices: 0.01 us -> 27 us  [on_device(): lax.all_to_all(grad_resid, 'sp', split_axis=1, concat_axis=0, tiled=True)]
    all_to_all x1 -> x0, blocking collectives: 26.8 us -> none  [on_device(): lax.all_to_all(summed.reshape(experts, capacity, -1), 'sp', split_axis=0,...]
    all_to_all x0 -> x3, starting transfers between devices: none -> 12.5 us  [the longest x1 5.51 us: on_device(): lax.all_to_all(summed.reshape(experts, capacity, -1), 'sp', split_axis=0,...]
  transfers between devices with their start and end apart: 7 -> 9, of which waited for: 6 -> 8; matrix products, arithmetic and copies ran while one was open for 8% -> 11% of each run, Pallas kernels for 2% -> 2%
where the time goes in v2:
time: 247 us; the launch traced here: 246 us
  waiting for transfers between devices  122 us (49%)
  blocking collectives  40.8 us (17%)
  matrix products  27.6 us (11%)
  starting transfers between devices  16.3 us (7%)
  between operations  15.6 us (6%)
  Pallas kernels  10.2 us (4%)
  local copies, waits for them, and re-layouts  6.88 us (3%)
  other arithmetic  6.46 us (3%)
    all_to_all x2, blocking collectives, on_device(): lax.all_to_all(rows.reshape(experts, capacity, -1), 'sp', split_axis=0, c...  34.3 us
    reduce_scatter x1, waiting for transfers between devices, on_device(): lax.psum_scatter(partial_short, 'tp', scatter_dimension=2, tiled=True)  27.6 us
    all_to_all x1, waiting for transfers between devices, on_device(): lax.all_to_all(grad_resid, 'sp', split_axis=1, concat_axis=0, tiled=True)  27 us
    all_to_all x1, waiting for transfers between devices, on_device(): lax.all_to_all(summed.reshape(experts, capacity, -1), 'sp', split_axis=0,...  20.6 us
    all_gather x1, waiting for transfers between devices, on_device(): lax.all_gather(arrived[1], 'tp', axis=2, tiled=True)  16.8 us
    all_gather x1, waiting for transfers between devices, on_device(): proj_all = lax.all_gather(out_proj, 'sp', axis=0, tiled=True)  15.5 us
    all_to_all x1, waiting for transfers between devices, on_device(): lax.all_to_all(own_rows.reshape(sp_count, heads * share, packed), 'sp', s...  10.3 us
    all_gather x1, blocking collectives, on_device(): lax.all_gather(lax.dot_general(slot_tokens, flat_rows, (((0,), (0,)), (()...  6.5 us
  transfers between devices with their start and end apart: 9, of which 8 were waited for; matrix products, arithmetic and copies ran while one was open for 11% of the time, Pallas kernels for 2%

profile of v2, /device:TPU:0, one launch (start us, length us, event | category | flops | bytes accessed | tf_op | source)
XLA Modules:
  0.0 245.6 jit_solution(101586564451020720)
XLA Ops:
  14.0 19.2 %all_to_all.44 = bf16[8,48,512]{2,1,0:T(8,128)(2,1)} all-to-all(bf16[8,48,512]{2,1,0:T(8,128)(2,1)S(1)} %bitcast.83), channel_id=1, replica_groups=mesh['sp'=8,'tp'=4] {'sp'}, dimensions={0} | all-to-all | bytes 786432 | tf_op jit(solution)/shard_map/all_to_all | solution.py:144
  34.9 15.1 %all_to_all.45 = bf16[8,48,512]{2,1,0:T(8,128)(2,1)} all-to-all(bf16[8,48,512]{2,1,0:T(8,128)(2,1)S(1)} %bitcast.84), channel_id=1, replica_groups=mesh['sp'=8,'tp'=4] {'sp'}, dimensions={0} | all-to-all | bytes 786432 | tf_op jit(solution)/shard_map/all_to_all | solution.py:144
  51.8 2.5 %fusion.6 = f32[384,512]{1,0:T(8,128)S(1)} fusion(bf16[1,2048,512]{2,1,0:T(8,128)(2,1)S(1)} %copy-done, bf16[1,384,2048]{2,1,0:T(8,128)(2,1)} %all-gather.5.cloned.1.call-done), kind=kOutput, calls=%fused_computation.10 | convolution fusion | flops 805306368 | bytes 4456448 | tf_op jit(solution)/shard_map/erd,edf->erf/dot_general | solution.py:154
  54.3 1.9 fusion.9
  56.2 16.8 %all-gather.7.cloned.1.call-done = bf16[1,384,2048]{2,1,0:T(8,128)(2,1)} async-done(((bf16[1,384,512]{2,1,0:T(8,128)(2,1)}), bf16[1,384,2048]{2,1,0:T(8,128)(2,1)}) %all-gather.7.cloned.1.call-update) | async-done | bytes 1572880 | tf_op jit(solution)/shard_map/all_gather | solution.py:152
  73.0 3.4 %multiply_convert_fusion.1 = (bf16[384,512]{1,0:T(8,128)(2,1)S(1)}, bf16[384,512]{1,0:T(8,128)(2,1)S(1)}) fusion(f32[384,512]{1,0:T(8,128)S(1)} %fusion.6, f32[384,512]{1,0:T(8,128)} %fusion.9, bf16[1,512,2048]{2,1,0:T(8,128)(2,1)} %param.22, bf16[1,384,2048]{2,1,0:T(8,128)(2,1)} %all-gather.7.cloned.1.call-done), kind=kOutput, calls=%fused_computation.34 | convolution fusion | flops 807862272 | bytes 6029312 | tf_op jit(solution)/shard_map/erd,efd->erf/dot_general | solution.py:160
  78.3 2.2 fusion.3
  81.1 27.6 %reduce-scatter.2.cloned.1.call-done = bf16[1,384,512]{2,1,0:T(8,128)(2,1)} async-done(((bf16[1,384,2048]{2,1,0:T(8,128)(2,1)}), bf16[1,384,512]{2,1,0:T(8,128)(2,1)}) %reduce-scatter.2.cloned.1.call-update) | async-done | bytes 393232 | tf_op jit(solution)/shard_map/reduce_scatter | solution.py:182
  108.7 5.5 %all-to-all-start.2 = ((bf16[8,48,512]{2,1,0:T(8,128)(2,1)}), bf16[8,48,512]{2,1,0:T(8,128)(2,1)S(1)}, u32[]{:S(2)}, u32[]{:S(2)}) async-start(bf16[8,48,512]{2,1,0:T(8,128)(2,1)} %bitcast.86), calls=%async_computation.3 | async-start | bytes 786432 | tf_op jit(solution)/shard_map/all_to_all | solution.py:186
  114.8 20.6 %all-to-all-done.2 = bf16[8,48,512]{2,1,0:T(8,128)(2,1)S(1)} async-done(((bf16[8,48,512]{2,1,0:T(8,128)(2,1)}), bf16[8,48,512]{2,1,0:T(8,128)(2,1)S(1)}, u32[]{:S(2)}, u32[]{:S(2)}) %all-to-all-start.2) | async-done | bytes 393248 | tf_op jit(solution)/shard_map/all_to_all | solution.py:186
  136.5 6.5 %all_gather.17 = bf16[128,2048]{1,0:T(8,128)(2,1)S(1)} all-gather(bf16[128,512]{1,0:T(8,128)(2,1)S(1)} %convolution_convert_fusion.4), channel_id=1, replica_groups=mesh['sp'=8,'tp'=4] {'tp'}, dimensions={1}, use_global_device_ids=true | all-gather | bytes 655360 | tf_op jit(solution)/shard_map/all_gather | solution.py:190
  144.5 15.5 %all-gather.11.cloned.1.call-done.proj_ref = bf16[2048,1024]{1,0:T(8,128)(2,1)} async-done(((bf16[256,1024]{1,0:T(8,128)(2,1)}), bf16[2048,1024]{1,0:T(8,128)(2,1)}) %all-gather.11.cloned.1.call-update) | async-done | bytes 4194320 | tf_op jit(solution)/shard_map/all_gather | solution.py:204
  160.0 5.6 %summary.1 = (bf16[128,1024]{1,0:T(8,128)(2,1)}, f32[128,512]{1,0:T(8,128)}, bf16[4,128,384]{2,1,0:T(8,128)(2,1)}) custom-call(bf16[128,2048]{1,0:T(8,128)(2,1)} %add_convert_fusion.1.resid_ref, bf16[2048,1024]{1,0:T(8,128)(2,1)} %all-gather.11.cloned.1.call-done.proj_ref, bf16[128,512]{1,0:T(8,128)(2,1)} %query_ref.3, f32[128,512]{1,0:T(8,128)} %decay_ref.1), custom_call_target="tpu_custom_call" | custom-call | flops 603979776 | bytes 5242880 | tf_op jit(solution)/shard_map/summary/pallas_call | solution.py:209
  165.6 1.8 copy.56
  167.4 3.5 %all-to-all-start.4 = ((bf16[8,64,384]{2,1,0:T(8,128)(2,1)}), bf16[8,64,384]{2,1,0:T(8,128)(2,1)S(1)}, u32[]{:S(2)}, u32[]{:S(2)}) async-start(bf16[8,64,384]{2,1,0:T(8,128)(2,1)} %bitcast.21), calls=%async_computation.5 | async-start | bytes 786432 | tf_op jit(solution)/shard_map/all_to_all | solution.py:233
  171.0 4.2 %fusion.1 = bf16[1,2048,512]{2,1,0:T(8,128)(2,1)} fusion(bf16[384,512]{1,0:T(8,128)(2,1)S(1)} %copy-done.8, bf16[1,384,2048]{2,1,0:T(8,128)(2,1)} %all-gather.5.cloned.1.call-done), kind=kOutput, calls=%fused_computation.5 | convolution fusion | flops 806354944 | bytes 4063232 | tf_op jit(solution)/shard_map/erd,erf->edf/dot_general | solution.py:171
  175.2 2.7 %fusion.2 = bf16[1,512,2048]{2,1,0:T(8,128)(2,1)} fusion(bf16[1,384,2048]{2,1,0:T(8,128)(2,1)S(1)} %copy-done.15, f32[384,512]{1,0:T(8,128)S(1)} %copy-done.18, f32[384,512]{1,0:T(8,128)S(1)} %copy-done.17), kind=kOutput, calls=%fused_computation.6 | convolution fusion | flops 807534592 | bytes 5242880 | tf_op jit(solution)/shard_map/erf,erd->efd/dot_general | solution.py:167
  178.7 10.3 %all-to-all-done.4 = bf16[8,64,384]{2,1,0:T(8,128)(2,1)S(1)} async-done(((bf16[8,64,384]{2,1,0:T(8,128)(2,1)}), bf16[8,64,384]{2,1,0:T(8,128)(2,1)S(1)}, u32[]{:S(2)}, u32[]{:S(2)}) %all-to-all-start.4) | async-done | bytes 393248 | tf_op jit(solution)/shard_map/all_to_all | solution.py:233
  189.0 3.6 %all-to-all-start.3 = ((bf16[128,8,256]{2,0,1:T(8,128)(2,1)}), bf16[128,8,256]{2,0,1:T(8,128)(2,1)S(1)}, u32[]{:S(2)}, u32[]{:S(2)}) async-start(bf16[128,8,256]{2,0,1:T(8,128)(2,1)} %bitcast.77), calls=%async_computation.4 | async-start | bytes 1048576 | tf_op jit(solution)/shard_map/all_to_all | solution.py:203
  194.2 27.0 %all-to-all-done.3 = bf16[128,8,256]{2,0,1:T(8,128)(2,1)S(1)} async-done(((bf16[128,8,256]{2,0,1:T(8,128)(2,1)}), bf16[128,8,256]{2,0,1:T(8,128)(2,1)S(1)}, u32[]{:S(2)}, u32[]{:S(2)}) %all-to-all-start.3) | async-done | bytes 524320 | tf_op jit(solution)/shard_map/all_to_all | solution.py:203
  221.3 3.4 %all-to-all-start.5 = ((bf16[8,64,256]{2,1,0:T(8,128)(2,1)}), bf16[8,64,256]{2,1,0:T(8,128)(2,1)S(1)}, u32[]{:S(2)}, u32[]{:S(2)}) async-start(bf16[8,64,256]{2,1,0:T(8,128)(2,1)} %copy-done.11), calls=%async_computation.6 | async-start | bytes 524288 | tf_op jit(solution)/shard_map/all_to_all | solution.py:246
  224.7 4.0 %fusion = bf16[1,2048,512]{2,1,0:T(8,128)(2,1)} fusion(bf16[384,512]{1,0:T(8,128)(2,1)S(1)} %copy-done.10, bf16[1,384,2048]{2,1,0:T(8,128)(2,1)} %all-gather.5.cloned.1.call-done), kind=kOutput, calls=%fused_computation.4 | convolution fusion | flops 806354944 | bytes 4063232 | tf_op jit(solution)/shard_map/erd,erf->edf/dot_general | solution.py:168
  228.7 3.3 %fusion.45 = f32[256,1024]{1,0:T(8,128)} fusion(bf16[1024,256]{1,0:T(8,128)(2,1)S(1)} %bitcast.79, bf16[1024,1024]{1,0:T(8,128)(2,1)} %all-gather.9.cloned.1.call-done), kind=kOutput, calls=%fused_computation.93 | convolution fusion | flops 536870912 | bytes 3670016 | tf_op jit(solution)/shard_map/dot_general | solution.py:284
  233.9 4.6 %gradients.1 = (bf16[128,512]{1,0:T(8,128)(2,1)}, bf16[128,512]{1,0:T(8,128)(2,1)}, bf16[128,1024]{1,0:T(8,128)(2,1)}, f32[128,512]{1,0:T(8,128)}) custom-call(bf16[4,128,256]{2,1,0:T(8,128)(2,1)} %bitcast.88, bf16[128,1024]{1,0:T(8,128)(2,1)} %get-tuple-element.16.grad_ref, bf16[128,512]{1,0:T(8,128)(2,1)} %query_ref.3, bf16[128,512]{1,0:T(8,128)(2,1)} %key_ref.1, ...), custom_call_target="tpu_custom_call" | custom-call | flops 671088640 | bytes 3407872 | tf_op jit(solution)/shard_map/gradients/pallas_call | solution.py:258
  (91 shorter events, 19.2 us)
Async XLA Ops:
  8.0 43.8 %copy-start = (bf16[1,2048,512]{2,1,0:T(8,128)(2,1)S(1)}, bf16[1,2048,512]{2,1,0:T(8,128)(2,1)}, u32[]{:S(2)}) copy-start(bf16[1,2048,512]{2,1,0:T(8,128)(2,1)} %param.20) | copy-start | bytes 6291460
  8.0 5.6 %copy-start.12 = (f32[2048]{0:T(1024)S(1)}, f32[2048]{0:T(1024)}, u32[]{:S(2)}) copy-start(f32[2048]{0:T(1024)} %param.16) | copy-start | bytes 24580
  8.0 43.8 %all-gather.5.cloned.1.call-start = ((), (), s32[]{:S(2)}) async-start(), calls=%async_computation.7 | async-start | bytes 1966080 | tf_op jit(solution)/shard_map/all_gather | solution.py:151
  10.2 23.1 %copy-start.13 = (f32[128,2]{0,1:T(2,128)S(1)}, f32[128,2]{0,1:T(2,128)}, u32[]{:S(2)}) copy-start(f32[128,2]{0,1:T(2,128)} %param.19) | copy-start | bytes 3076
  11.2 23.7 %copy-start.6 = (pred[384,128]{1,0:T(8,128)(4,1)}, pred[384,128]{1,0:T(8,128)(4,1)S(1)}, u32[]{:S(2)}) copy-start(pred[384,128]{1,0:T(8,128)(4,1)S(1)} %fusion.22) | copy-start | bytes 147460
  33.3 39.7 %all-gather.7.cloned.1.call-start = ((), (), s32[]{:S(2)}) async-start(), calls=%async_computation.8 | async-start | bytes 1966080 | tf_op jit(solution)/shard_map/all_gather | solution.py:152
  50.0 58.6 %reduce-scatter.2.cloned.1.call-start = ((), (), s32[]{:S(2)}) async-start(), calls=%async_computation.9 | async-start | bytes 1966080 | tf_op jit(solution)/shard_map/reduce_scatter | solution.py:182
  51.8 2.5 %copy-start.3 = (bf16[1,2048,512]{2,1,0:T(8,128)(2,1)S(1)}, bf16[1,2048,512]{2,1,0:T(8,128)(2,1)}, u32[]{:S(2)}) copy-start(bf16[1,2048,512]{2,1,0:T(8,128)(2,1)} %param.21) | copy-start | bytes 6291460
  51.8 2.5 %copy-start.14 = (bf16[1,384,2048]{2,1,0:T(8,128)(2,1)S(1)}, bf16[1,384,2048]{2,1,0:T(8,128)(2,1)}, u32[]{:S(2)}) copy-start(bf16[1,384,2048]{2,1,0:T(8,128)(2,1)} %all-gather.5.cloned.1.call-done) | copy-start | bytes 4718596
  54.3 18.7 %copy-start.16 = (f32[384,512]{1,0:T(8,128)}, f32[384,512]{1,0:T(8,128)S(1)}, u32[]{:S(2)}) copy-start(f32[384,512]{1,0:T(8,128)S(1)} %fusion.6) | copy-start | bytes 2359300
  80.5 62.5 %copy-start.1 = (bf16[128,2048]{1,0:T(8,128)(2,1)S(1)}, bf16[128,2048]{1,0:T(8,128)(2,1)}, u32[]{:S(2)}) copy-start(bf16[128,2048]{1,0:T(8,128)(2,1)} %param.15) | copy-start | bytes 1572868
  80.5 62.8 %copy-start.5 = (bf16[128,2048]{1,0:T(8,128)(2,1)S(1)}, bf16[128,2048]{1,0:T(8,128)(2,1)}, u32[]{:S(2)}) copy-start(bf16[128,2048]{1,0:T(8,128)(2,1)} %param.17) | copy-start | bytes 1572868
  80.5 79.5 %all-gather.11.cloned.1.call-start = ((), (), s32[]{:S(2)}) async-start(), calls=%async_computation.11 | async-start | bytes 4718592 | tf_op jit(solution)/shard_map/all_gather | solution.py:204
  108.7 26.7 %all-to-all-start.2 = ((bf16[8,48,512]{2,1,0:T(8,128)(2,1)}), bf16[8,48,512]{2,1,0:T(8,128)(2,1)S(1)}, u32[]{:S(2)}, u32[]{:S(2)}) async-start(bf16[8,48,512]{2,1,0:T(8,128)(2,1)} %bitcast.86), calls=%async_computation.3 | async-start | bytes 786432 | tf_op jit(solution)/shard_map/all_to_all | solution.py:186
  114.2 114.5 %all-gather.9.cloned.1.call-start = ((), (), s32[]{:S(2)}) async-start(), calls=%async_computation.10 | async-start | bytes 2359296 | tf_op jit(solution)/shard_map/all_gather | solution.py:149
  144.5 26.4 %copy-start.8 = (bf16[384,512]{1,0:T(8,128)(2,1)S(1)}, bf16[384,512]{1,0:T(8,128)(2,1)}, u32[]{:S(2)}) copy-start(bf16[384,512]{1,0:T(8,128)(2,1)} %copy-done.7) | copy-start | bytes 1179652
  167.4 21.6 %all-to-all-start.4 = ((bf16[8,64,384]{2,1,0:T(8,128)(2,1)}), bf16[8,64,384]{2,1,0:T(8,128)(2,1)S(1)}, u32[]{:S(2)}, u32[]{:S(2)}) async-start(bf16[8,64,384]{2,1,0:T(8,128)(2,1)} %bitcast.21), calls=%async_computation.5 | async-start | bytes 786432 | tf_op jit(solution)/shard_map/all_to_all | solution.py:233
  170.9 4.2 %copy-start.15 = (bf16[1,384,2048]{2,1,0:T(8,128)(2,1)S(1)}, bf16[1,384,2048]{2,1,0:T(8,128)(2,1)}, u32[]{:S(2)}) copy-start(bf16[1,384,2048]{2,1,0:T(8,128)(2,1)} %all-gather.7.cloned.1.call-done) | copy-start | bytes 4718596
  170.9 4.2 %copy-start.17 = (f32[384,512]{1,0:T(8,128)S(1)}, f32[384,512]{1,0:T(8,128)}, u32[]{:S(2)}) copy-start(f32[384,512]{1,0:T(8,128)} %copy-done.16) | copy-start | bytes 2359300
  171.0 4.2 %copy-start.18 = (f32[384,512]{1,0:T(8,128)S(1)}, f32[384,512]{1,0:T(8,128)}, u32[]{:S(2)}) copy-start(f32[384,512]{1,0:T(8,128)} %fusion.9) | copy-start | bytes 2359300
  175.2 2.7 %copy-start.2 = (bf16[128,2048]{1,0:T(8,128)(2,1)S(1)}, bf16[128,2048]{1,0:T(8,128)(2,1)}, u32[]{:S(2)}) copy-start(bf16[128,2048]{1,0:T(8,128)(2,1)} %add_convert_fusion.1.resid_ref) | copy-start | bytes 1572868
  189.0 35.7 %copy-start.10 = (bf16[384,512]{1,0:T(8,128)(2,1)S(1)}, bf16[384,512]{1,0:T(8,128)(2,1)}, u32[]{:S(2)}) copy-start(bf16[384,512]{1,0:T(8,128)(2,1)} %copy-done.9) | copy-start | bytes 1179652
  189.0 32.3 %all-to-all-start.3 = ((bf16[128,8,256]{2,0,1:T(8,128)(2,1)}), bf16[128,8,256]{2,0,1:T(8,128)(2,1)S(1)}, u32[]{:S(2)}, u32[]{:S(2)}) async-start(bf16[128,8,256]{2,0,1:T(8,128)(2,1)} %bitcast.77), calls=%async_computation.4 | async-start | bytes 1048576 | tf_op jit(solution)/shard_map/all_to_all | solution.py:203
  221.3 11.9 %all-to-all-start.5 = ((bf16[8,64,256]{2,1,0:T(8,128)(2,1)}), bf16[8,64,256]{2,1,0:T(8,128)(2,1)S(1)}, u32[]{:S(2)}, u32[]{:S(2)}) async-start(bf16[8,64,256]{2,1,0:T(8,128)(2,1)} %copy-done.11), calls=%async_computation.6 | async-start | bytes 524288 | tf_op jit(solution)/shard_map/all_to_all | solution.py:246
  (4 other events, 4.7 us)
Sparse Core Ops, SparseCore 0:
  33.4 18.3 all-gather.4
  53.3 19.6 all-gather.6
  80.7 27.9 reduce-scatter.1
Sparse Core Ops, SparseCore 1:
  83.2 76.8 all-gather.10
  162.0 61.8 all-gather.8
